TPU v7x, 32 devices: a whole 2x2x4 slice. The times are simulated.
32 devices in a mesh: sp: 16 (over z, y, x), tp: 2 (over core).
Axes of the slice: x: 2, y: 2, z: 4, core: 2. Of those that a mesh axis runs over, the one named last changes fastest.
Arguments:
- resid: bfloat16 [6144, 2048], P(('sp', 'tp')), may hold values from -6 to 6
- q_small: bfloat16 [6144, 1024], P('sp', 'tp'), may hold values from -6 to 6
- k_small: bfloat16 [6144, 1024], P('sp', 'tp'), may hold values from -6 to 6
- v_small: bfloat16 [6144, 1024], P('sp', 'tp'), may hold values from -6 to 6
- q_large: bfloat16 [6144, 1024], P('sp', 'tp'), may hold values from -6 to 6
- k_large: bfloat16 [6144, 1024], P('sp', 'tp'), may hold values from -6 to 6
- v_large: bfloat16 [6144, 1024], P('sp', 'tp'), may hold values from -6 to 6
- gate_small: bfloat16 [6144, 1024], P('sp', 'tp'), may hold values from -6 to 6
- large_head_gate: bfloat16 [6144, 1024], P('sp', 'tp'), may hold values from -6 to 6
- gates_small: float32 [6144, 3, 16], P('sp', None, 'tp'), may hold values from -6 to 300, as said below
- gates_large: float32 [6144, 3, 8], P('sp', None, 'tp'), may hold values from -6 to 300, as said below
- w_out_small: bfloat16 [1024, 2048], P('tp'), may hold values from -0.125 to 0.125
- w_out_large: bfloat16 [1024, 2048], P('tp'), may hold values from -0.125 to 0.125
- norm_gain: float32 [2048], replicated, may hold values from 0.1 to 1.9
- expert_ids: int32 [6144, 2], P(('sp', 'tp')), may hold values from 0 to 15, all different within a row; in each aligned block of 192 rows (0 to 191, 192 to 383, ...) at most 48 rows name the same one
- expert_weight: float32 [6144, 2], P(('sp', 'tp')), may hold values from 0.2 to 1
- w_gate: bfloat16 [16, 2048, 2048], P('sp', None, 'tp'), may hold values from -0.125 to 0.125
- w_up: bfloat16 [16, 2048, 2048], P('sp', None, 'tp'), may hold values from -0.125 to 0.125
- w_down: bfloat16 [16, 2048, 2048], P('sp', 'tp'), may hold values from -0.125 to 0.125
Outputs:
- layer_out: bfloat16 [6144, 2048], P(('sp', 'tp'))
Inputs may be any that keep to these rules, and one draw needn't show every extreme that they name: `gates_small`: field 0 is the input gate's pre-activation, field 1 the forget gate's pre-activation, field 2 a non-positive term added to the log forget gate. `gates_large`: field 0 is the input gate's pre-activation, field 1 the forget gate's pre-activation, field 2 a non-positive term added to the log forget gate. `expert_ids`: each row names 2 different experts. In the 192 rows of one device no expert is named by more than 48 rows, and in some device's rows an expert is named exactly 48 times.
All inputs are finite; a program needn't handle non-finite values.
Results may differ from a plain program's by a relative error of at most 0.014.
Values may be sent and summed in bfloat16 or wider, within the bound.
A program may use at most 128 MiB of HBM per device.

v0:
```python
import jax
import jax.numpy as jnp
from jax import lax
from jax.sharding import PartitionSpec as P

floor_neg = -1e30
norm_eps = 1e-06


def carried_in(x, axis, combine, identity):
    peers, here = (lax.axis_size(axis), lax.axis_index(axis))
    everything = jax.tree.map(lambda part: lax.all_gather(part, axis), x)
    start = jax.tree.map(
        lambda part, zero: jnp.broadcast_to(jnp.asarray(zero, part.dtype), part.shape), x, identity
    )

    def lap(k, before):
        reached = k < here
        new = combine(before, jax.tree.map(lambda part: part[k], everything))
        return jax.tree.map(lambda a, b: jnp.where(reached, a, b), new, before)

    return lax.fori_loop(0, peers, lap, start)


def summarize(keys_block, values_block, log_in, log_forget):
    cumulative = jnp.cumsum(log_forget, axis=0)
    totals = cumulative[-1]
    growth = totals[None, :] - cumulative + log_in
    peak_log = jnp.max(growth, axis=0)
    factor = jnp.exp(growth - peak_log[None, :])
    scaled = factor[:, :, None] * keys_block.astype(jnp.float32)
    keyed_rows = scaled.astype(jnp.bfloat16)
    state_mat = jnp.einsum(
        "lhd,lhe->hde", keyed_rows, values_block, preferred_element_type=jnp.float32
    )
    state_vec = jnp.sum(scaled, axis=0)
    return (state_mat, state_vec, peak_log, totals)


def combine(earlier, later):
    earlier_mat, earlier_vec, earlier_peak, earlier_total = earlier
    later_mat, later_vec, later_peak, later_total = later
    joined = jnp.maximum(earlier_peak + later_total, later_peak)
    earlier_weight = jnp.exp(earlier_peak + later_total - joined)
    later_weight = jnp.exp(later_peak - joined)
    return (
        earlier_weight[:, None, None] * earlier_mat + later_weight[:, None, None] * later_mat,
        earlier_weight[:, None] * earlier_vec + later_weight[:, None] * later_vec,
        joined,
        earlier_total + later_total,
    )


def combine_groups(earlier, later):
    return combine(earlier[:4], later[:4]) + combine(earlier[4:], later[4:])


def blank_state(head_count, head_dim):
    return (
        jnp.zeros((head_count, head_dim, head_dim), jnp.float32),
        jnp.zeros((head_count, head_dim), jnp.float32),
        jnp.full((head_count,), floor_neg, jnp.float32),
        jnp.zeros((head_count,), jnp.float32),
    )


def read_block(queries, keys_block, values_block, log_in, log_forget, carried):
    state_mat, state_vec, carry_peak, carry_total = carried
    length = queries.shape[0]
    scaling = queries.shape[2] ** (-0.5)
    cumulative = jnp.cumsum(log_forget, axis=0).T
    entries = log_in.T
    positions = jnp.arange(length)
    causal = positions[:, None] >= positions[None, :]
    dlog = jnp.where(
        causal[None],
        cumulative[:, :, None] - cumulative[:, None, :] + entries[:, None, :],
        floor_neg,
    )
    carried_log = cumulative + carry_peak[:, None]
    ceiling = jnp.maximum(carried_log, jnp.max(dlog, axis=2))
    products = (
        jnp.einsum("thd,shd->hts", queries, keys_block, preferred_element_type=jnp.float32)
        * scaling
    )
    scored = products * jnp.exp(dlog - ceiling[:, :, None])
    scored_b = scored.astype(jnp.bfloat16)
    carry_weight = jnp.exp(carried_log - ceiling)
    scaled_queries = queries.astype(jnp.float32) * scaling
    numerator = jnp.einsum(
        "hts,shd->htd", scored_b, values_block, preferred_element_type=jnp.float32
    )
    numerator = numerator + carry_weight[:, :, None] * jnp.einsum(
        "thd,hde->hte", scaled_queries, state_mat, precision=lax.Precision.HIGHEST
    )
    denominator = jnp.sum(scored, axis=2) + carry_weight * jnp.einsum(
        "thd,hd->ht", scaled_queries, state_vec, precision=lax.Precision.HIGHEST
    )
    memory = numerator / jnp.maximum(jnp.abs(denominator), 1.0)[:, :, None]
    return jnp.transpose(memory, (1, 0, 2))


def split_heads(queries, keys, values, gates):
    head_count = gates.shape[2]
    head_dim = queries.shape[1] // head_count
    length = queries.shape[0]
    shaped = tuple(
        (array.reshape(length, head_count, head_dim) for array in (queries, keys, values))
    )
    log_in = gates[:, 0, :]
    log_forget = jax.nn.log_sigmoid(gates[:, 1, :]) + gates[:, 2, :]
    return (shaped, log_in, log_forget)


def gated_output(out_gate, memory):
    flattened = memory.reshape(memory.shape[0], -1)
    return (jax.nn.sigmoid(out_gate.astype(jnp.float32)) * flattened).astype(jnp.bfloat16)


def expert_part(arrived, gate_w, up_w, down_w):
    gated = jnp.dot(arrived, gate_w, preferred_element_type=jnp.float32)
    lifted = jnp.dot(arrived, up_w, preferred_element_type=jnp.float32)
    hidden = (jax.nn.silu(gated) * lifted).astype(jnp.bfloat16)
    return jnp.dot(hidden, down_w, preferred_element_type=jnp.float32)


def body(
    resid,
    q_small,
    k_small,
    v_small,
    q_large,
    k_large,
    v_large,
    gate_small,
    large_head_gate,
    gates_small,
    gates_large,
    w_out_small,
    w_out_large,
    norm_gain,
    expert_ids,
    expert_weight,
    w_gate,
    w_up,
    w_down,
):
    tok_dev = q_small.shape[0]
    small_heads, small_in, small_forget = split_heads(q_small, k_small, v_small, gates_small)
    large_heads, broad_input_vector, large_forget = split_heads(
        q_large, k_large, v_large, gates_large
    )
    small_mat, small_vec, small_peak, small_total = summarize(
        small_heads[1], small_heads[2], small_in, small_forget
    )
    large_mat, large_vec, large_peak, large_total = summarize(
        large_heads[1], large_heads[2], broad_input_vector, large_forget
    )
    identity = blank_state(small_heads[0].shape[1], small_heads[0].shape[2]) + blank_state(
        large_heads[0].shape[1], large_heads[0].shape[2]
    )
    carried = carried_in(
        (
            small_mat,
            small_vec,
            small_peak,
            small_total,
            large_mat,
            large_vec,
            large_peak,
            large_total,
        ),
        "sp",
        combine_groups,
        identity,
    )
    small_memory = read_block(
        small_heads[0], small_heads[1], small_heads[2], small_in, small_forget, carried[:4]
    )
    large_memory = read_block(
        large_heads[0],
        large_heads[1],
        large_heads[2],
        broad_input_vector,
        large_forget,
        carried[4:],
    )
    small_out = gated_output(gate_small, small_memory)
    large_out = gated_output(large_head_gate, large_memory)
    row_count = tok_dev // lax.axis_size("tp")
    mixed = lax.psum_scatter(
        (
            jnp.dot(small_out, w_out_small, preferred_element_type=jnp.float32)
            + jnp.dot(large_out, w_out_large, preferred_element_type=jnp.float32)
        ).astype(jnp.bfloat16),
        "tp",
        scatter_dimension=0,
        tiled=True,
    ).astype(jnp.float32)
    after_mix = resid.astype(jnp.float32) + mixed
    normed = (
        after_mix
        * lax.rsqrt(jnp.mean(after_mix * after_mix, axis=-1, keepdims=True) + norm_eps)
        * norm_gain
    ).astype(jnp.bfloat16)
    features = normed.shape[1]
    top_count = expert_ids.shape[1]
    num_experts = w_gate.shape[0] * lax.axis_size("sp")
    capacity = max(2, tok_dev * top_count // num_experts)
    routed = expert_ids.reshape(-1)
    route_total = routed.shape[0]
    onehot = (routed[:, None] == jnp.arange(num_experts, dtype=jnp.int32)[None, :]).astype(
        jnp.int32
    )
    position = jnp.sum((jnp.cumsum(onehot, axis=0) - 1) * onehot, axis=1)
    slot_index = routed * capacity + position
    source_rows = normed[jnp.arange(route_total) // top_count]
    outgoing = (
        jnp.zeros((num_experts * capacity, features), jnp.bfloat16).at[slot_index].set(source_rows)
    )
    outgoing = outgoing.reshape(num_experts, capacity, features)
    own_gate = w_gate[0]
    private_lifting_matrix = w_up[0]
    own_down = w_down[0]
    complete_gate, full_up = (
        lax.all_gather(own_gate, "tp", axis=1, tiled=True),
        lax.all_gather(private_lifting_matrix, "tp", axis=1, tiled=True),
    )
    full_down = lax.all_gather(own_down, "tp", axis=0, tiled=True)
    part_width = own_gate.shape[1]
    arrived = lax.all_to_all(outgoing, "sp", split_axis=0, concat_axis=0, tiled=True)
    flattened = arrived.reshape(-1, features)
    running = jnp.zeros(flattened.shape, jnp.float32)
    for member in range(lax.axis_size("tp")):
        low = member * part_width
        portion = expert_part(
            flattened,
            complete_gate[:, low : low + part_width],
            full_up[:, low : low + part_width],
            full_down[low : low + part_width],
        )
        running = running + lax.optimization_barrier(portion.astype(jnp.bfloat16)).astype(
            jnp.float32
        )
    answered = running.astype(jnp.bfloat16).reshape(arrived.shape)
    returned = lax.all_to_all(answered, "sp", split_axis=0, concat_axis=0, tiled=True)
    picked = returned.reshape(num_experts * capacity, features)[slot_index]
    weighted = picked.astype(jnp.float32) * expert_weight.reshape(-1)[:, None]
    combined = jnp.sum(weighted.reshape(row_count, top_count, features), axis=1)
    return (after_mix + combined).astype(jnp.bfloat16)


def solution(mesh):
    return jax.shard_map(
        body,
        mesh=mesh,
        in_specs=(
            P(("sp", "tp"), None),
            P("sp", "tp"),
            P("sp", "tp"),
            P("sp", "tp"),
            P("sp", "tp"),
            P("sp", "tp"),
            P("sp", "tp"),
            P("sp", "tp"),
            P("sp", "tp"),
            P("sp", None, "tp"),
            P("sp", None, "tp"),
            P("tp", None),
            P("tp", None),
            P(),
            P(("sp", "tp"), None),
            P(("sp", "tp"), None),
            P("sp", None, "tp"),
            P("sp", None, "tp"),
            P("sp", "tp", None),
        ),
        out_specs=P(("sp", "tp"), None),
        check_vma=False,
    )
```

profile of v0, /device:TPU:12, one launch (start us, length us, event | category | flops | bytes accessed | tf_op | source)
XLA Modules:
  0.0 632.7 jit_solution(14547233404910226935)
XLA Ops:
  19.6 2.0 fusion.54
  24.8 32.4 %all-reduce.2 = (f32[128]{0:T(128)S(1)}, f32[64]{0:T(128)S(1)}) all-reduce(f32[128]{0:T(128)S(1)} %dynamic-update-slice, f32[64]{0:T(128)S(1)} %dynamic-update-slice.1), channel_id=2, replica_groups=mesh['sp'=16,'tp'=2] {'sp'}, use_global_device_ids=true, to_apply=%add | all-reduce | flops 192 | bytes 1536
  59.5 2.3 copy.109
  61.9 1.9 copy.72
  63.8 35.9 %all-gather.8 = f32[16,1,4]{2,1,0:T(1,128)} all-gather(f32[1,1,4]{2,1,0:T(1,128)S(1)} %bitcast.340), channel_id=1, replica_groups=mesh['sp'=16,'tp'=2] {'sp'}, dimensions={0}, use_global_device_ids=true | all-gather | bytes 272 | tf_op jit(solution)/shard_map/all_gather | solution.py:12
  99.7 40.3 %all-gather.7 = f32[16,1,8]{2,1,0:T(1,128)} all-gather(f32[1,1,8]{2,1,0:T(1,128)S(1)} %bitcast.339), channel_id=1, replica_groups=mesh['sp'=16,'tp'=2] {'sp'}, dimensions={0}, use_global_device_ids=true | all-gather | bytes 544 | tf_op jit(solution)/shard_map/all_gather | solution.py:12
  140.0 1.4 multiply_reduce_fusion.2
  141.4 39.1 %all_gather.58 = f32[16,4,128]{2,1,0:T(4,128)} all-gather(f32[1,4,128]{2,1,0:T(4,128)S(1)} %bitcast.338), channel_id=1, replica_groups=mesh['sp'=16,'tp'=2] {'sp'}, dimensions={0}, use_global_device_ids=true | all-gather | bytes 34816 | tf_op jit(solution)/shard_map/all_gather | solution.py:12
  180.5 39.3 %all_gather.52 = f32[16,8,64]{2,1,0:T(8,128)} all-gather(f32[1,8,64]{2,1,0:T(8,128)S(1)} %all_gather.51), channel_id=1, replica_groups=mesh['sp'=16,'tp'=2] {'sp'}, dimensions={0}, use_global_device_ids=true | all-gather | bytes 34816 | tf_op jit(solution)/shard_map/all_gather | solution.py:12
  221.1 1.9 fusion.29
  224.3 2.6 fusion.14
  226.8 139.7 %while.24 = (s32[]{:T(128)}, f32[8,64,64]{2,1,0:T(8,128)S(1)}, f32[8,64]{1,0:T(8,128)}, f32[8]{0:T(128)}, f32[4,128,128]{2,1,0:T(8,128)S(1)}, /*index=5*/f32[4,1...) while((s32[]{:T(128)}, f32[8,64,64]{2,1,0:T(8,128)S(1)}, ...), condition=%wide.region_9.10_spmd.clone, body=%wide.region_8.9_spmd.clone.sunk | while | flops 496728 | bytes 1192787 | solution.py:22
  241.5 1.4 fusion.141
  250.3 1.4 fusion.141
  259.0 1.4 fusion.141
  267.7 1.4 fusion.141
  276.4 1.4 fusion.141
  285.2 1.4 fusion.141
  293.9 1.4 fusion.141
  302.6 1.4 fusion.141
  311.4 1.4 fusion.141
  320.1 1.4 fusion.141
  367.4 2.3 fusion.111
  371.3 2.0 fusion.48
  373.3 2.3 copy.93
  376.4 3.0 fusion.27
  380.2 1.9 fusion.40
  384.3 2.3 fusion.55
  386.6 2.3 add_convert_fusion.1
  392.2 13.0 %reduce-scatter.2.cloned.1.call-done = bf16[192,2048]{1,0:T(8,128)(2,1)} async-done(((bf16[384,2048]{1,0:T(8,128)(2,1)}), bf16[192,2048]{1,0:T(8,128)(2,1)}) %reduce-scatter.2.cloned.1.call-update) | async-done | bytes 786448 | tf_op jit(solution)/shard_map/reduce_scatter | solution.py:191
  405.2 1.5 multiply_reduce_fusion.1
  406.7 1.5 multiply_convert_fusion.2
  408.2 10.0 %scatter_custom_fusion = bf16[768,2048]{1,0:T(8,128)(2,1)} fusion(s32[384]{0:T(512)S(1)} %fusion.95, bf16[192,2048]{1,0:T(8,128)(2,1)S(1)} %multiply_convert_fusion.2, s32[1024]{0:T(1024)S(1)} %pad_clamp_fusion.1, bf16[]{:T(256)} %constant.96.clone.1), kind=kCustom, calls=%fused_computation.62 | custom fusion | bytes 3145730 | tf_op jit(solution)/shard_map/scatter | solution.py:219
  418.2 7.0 %all-to-all-start = ((bf16[16,48,2048]{2,1,0:T(8,128)(2,1)}), bf16[16,48,2048]{2,1,0:T(8,128)(2,1)S(1)}, u32[]{:S(2)}, u32[]{:S(2)}) async-start(bf16[16,48,2048]{2,1,0:T(8,128)(2,1)} %bitcast.45), calls=%async_computation.1 | async-start | bytes 6291456 | tf_op jit(solution)/shard_map/all_to_all | solution.py:231
  425.8 1.9 all-gather.21.cloned.1.call-done
  427.7 68.9 %all-to-all-done = bf16[16,48,2048]{2,1,0:T(8,128)(2,1)S(1)} async-done(((bf16[16,48,2048]{2,1,0:T(8,128)(2,1)}), bf16[16,48,2048]{2,1,0:T(8,128)(2,1)S(1)}, u32[]{:S(2)}, u32[]{:S(2)}) %all-to-all-start) | async-done | bytes 3145760 | tf_op jit(solution)/shard_map/all_to_all | solution.py:231
  496.6 7.5 %fusion.21 = f32[768,1024]{1,0:T(8,128)} fusion(bf16[768,2048]{1,0:T(8,128)(2,1)S(1)} %bitcast.315, bf16[2048,2048]{1,0:T(8,128)(2,1)} %bitcast.346), kind=kOutput, calls=%fused_computation.45 | convolution fusion | flops 3221225472 | bytes 10485760 | tf_op jit(solution)/shard_map/dot_general | solution.py:122
  504.1 5.1 fusion.16
  509.2 7.5 %multiply_convert_fusion.1 = bf16[768,1024]{1,0:T(8,128)(2,1)} fusion(f32[768,1024]{1,0:T(8,128)} %fusion.21, bf16[768,2048]{1,0:T(8,128)(2,1)S(1)} %bitcast.317, bf16[2048,2048]{1,0:T(8,128)(2,1)} %bitcast.344), kind=kOutput, calls=%fused_computation.53 | convolution fusion | flops 3225944064 | bytes 12058624 | tf_op jit(solution)/shard_map/dot_general | solution.py:121
  516.7 6.2 fusion.25
  523.0 3.9 multiply_convert_fusion
  526.9 3.7 fusion.26
  530.6 3.1 add_convert_fusion
  533.7 6.1 all-to-all-start.1
  539.9 69.6 %all-to-all-done.1 = bf16[16,48,2048]{2,1,0:T(8,128)(2,1)S(1)} async-done(((bf16[16,48,2048]{2,1,0:T(8,128)(2,1)}), bf16[16,48,2048]{2,1,0:T(8,128)(2,1)S(1)}, u32[]{:S(2)}, u32[]{:S(2)}) %all-to-all-start.1) | async-done | bytes 3145760 | tf_op jit(solution)/shard_map/all_to_all | solution.py:246
  609.5 3.1 gather_fusion
  612.6 4.7 reshape.357
  617.4 7.0 %multiply_reduce_fusion = f32[192,2048]{1,0:T(8,128)S(1)} fusion(f32[192,2,2048]{2,1,0:T(2,128)} %reshape.357, f32[192,2]{1,0:T(8,128)S(1)} %copy.98), kind=kLoop, calls=%fused_computation.51 | loop fusion | flops 1179648 | bytes 4720128 | tf_op jit(solution)/shard_map/reduce_sum | solution.py:249
  (279 shorter events, 156.8 us)
Async XLA Ops:
  6.5 377.7 %copy-start = (bf16[512,2048]{1,0:T(8,128)(2,1)S(1)}, bf16[512,2048]{1,0:T(8,128)(2,1)}, u32[]{:S(2)}) copy-start(bf16[512,2048]{1,0:T(8,128)(2,1)} %param.32) | copy-start | bytes 6291460
  6.5 12.8 %copy-start.20 = (f32[384,3,4]{0,2,1:T(4,128)S(1)}, f32[384,3,4]{0,2,1:T(4,128)}, u32[]{:S(2)}) copy-start(f32[384,3,4]{0,2,1:T(4,128)} %param.31) | copy-start | bytes 55300
  6.5 10.4 %copy-start.9 = (bf16[384,512]{1,0:T(8,128)(2,1)S(1)}, bf16[384,512]{1,0:T(8,128)(2,1)}, u32[]{:S(2)}) copy-start(bf16[384,512]{1,0:T(8,128)(2,1)} %param.26) | copy-start | bytes 1179652
  6.5 220.3 %all-gather.15.cloned.1.call-start = ((), (), s32[]{:S(2)}) async-start(), calls=%async_computation.4 | async-start | bytes 4456448 | tf_op jit(solution)/shard_map/all_gather | solution.py:12
  11.1 11.4 %copy-start.33 = (u32[32]{0:T(128)S(1)}, u32[32]{0:T(128)}, u32[]{:S(2)}) copy-start(u32[32]{0:T(128)} %constant.109) | copy-start | bytes 388
  13.5 8.2 %copy-start.7 = (bf16[384,512]{0,1:T(8,128)(2,1)}, bf16[384,512]{0,1:T(8,128)(2,1)S(1)}, u32[]{:S(2)}) copy-start(bf16[384,512]{0,1:T(8,128)(2,1)S(1)} %copy.75) | copy-start | bytes 1179652
  14.5 212.3 %all-gather.17.cloned.1.call-start = ((), (), s32[]{:S(2)}) async-start(), calls=%async_computation.5 | async-start | bytes 4456448 | tf_op jit(solution)/shard_map/all_gather | solution.py:12
  17.0 46.9 %copy-start.10 = (f32[1,4,3,128]{3,2,1,0:T(4,128)}, f32[1,4,3,128]{3,2,1,0:T(4,128)S(1)}, u32[]{:S(2)}) copy-start(f32[1,4,3,128]{3,2,1,0:T(4,128)S(1)} %add_bitcast_fusion.3) | copy-start | bytes 18436
  21.6 383.6 %reduce-scatter.2.cloned.1.call-start = ((), (), s32[]{:S(2)}) async-start(), calls=%async_computation.3 | async-start | bytes 2359296 | tf_op jit(solution)/shard_map/reduce_scatter | solution.py:191
  220.5 0.6 copy-start.25
  223.7 0.6 copy-start.21
  367.4 2.4 copy-start.19
  367.4 2.4 copy-start.31
  367.4 3.8 copy-start.11
  367.4 3.8 copy-start.18
  367.4 3.8 copy-start.24
  371.2 5.3 copy-start.13
  376.4 3.0 copy-start.17
  376.4 3.7 copy-start.8
  376.4 3.7 copy-start.15
  376.4 3.7 copy-start.22
  380.1 1.9 copy-start.16
  380.1 1.9 copy-start.23
  380.2 2.0 copy-start.14
  382.0 2.2 copy-start.32
  384.3 2.3 copy-start.5
  384.3 2.3 copy-start.6
  384.3 2.3 copy-start.12
  388.9 38.8 %all-gather.21.cloned.1.call-start = ((), (), s32[]{:S(2)}) async-start(), calls=%async_computation.7 | async-start | bytes 12582912 | tf_op jit(solution)/shard_map/all_gather | solution.py:227
  389.5 0.7 copy-start.27
  389.5 15.7 %copy-start.2 = (bf16[192,2048]{1,0:T(8,128)(2,1)S(1)}, bf16[192,2048]{1,0:T(8,128)(2,1)}, u32[]{:S(2)}) copy-start(bf16[192,2048]{1,0:T(8,128)(2,1)} %param.21) | copy-start | bytes 2359300
  389.5 17.2 %copy-start.26 = (f32[2048]{0:T(1024)S(1)}, f32[2048]{0:T(1024)}, u32[]{:S(2)}) copy-start(f32[2048]{0:T(1024)} %param.34) | copy-start | bytes 24580
  389.5 119.7 %all-gather.19.cloned.1.call-start = ((), (), s32[]{:S(2)}) async-start(), calls=%async_computation.6 | async-start | bytes 12582912 | tf_op jit(solution)/shard_map/all_gather | solution.py:226
  418.2 78.3 %all-to-all-start = ((bf16[16,48,2048]{2,1,0:T(8,128)(2,1)}), bf16[16,48,2048]{2,1,0:T(8,128)(2,1)S(1)}, u32[]{:S(2)}, u32[]{:S(2)}) async-start(bf16[16,48,2048]{2,1,0:T(8,128)(2,1)} %bitcast.45), calls=%async_computation.1 | async-start | bytes 6291456 | tf_op jit(solution)/shard_map/all_to_all | solution.py:231
  425.2 91.5 %all-gather.23.cloned.1.call-start = ((), (), s32[]{:S(2)}) async-start(), calls=%async_computation.8 | async-start | bytes 12582912 | tf_op jit(solution)/shard_map/all_gather | solution.py:229
  496.6 7.5 %copy-start.30 = (bf16[1,2048,2048]{2,1,0:T(8,128)(2,1)S(1)}, bf16[1,2048,2048]{2,1,0:T(8,128)(2,1)}, u32[]{:S(2)}) copy-start(bf16[1,2048,2048]{2,1,0:T(8,128)(2,1)} %all-gather.21.cloned.1.call-done) | copy-start | bytes 25165828
  516.7 6.3 copy-start.29
  516.7 6.3 copy-start.34
  516.7 10.1 %slice-start = ((s8[8388608]{0:T(1024)(128)(4,1)}), s8[4194304]{0:T(1024)(128)(4,1)S(1)}, s32[]{:S(2)}) async-start(s8[8388608]{0:T(1024)(128)(4,1)} %bitcast.348), calls=%async_computation.9 | async-start | bytes 8388608
  523.0 3.9 slice-start.1
  533.7 6.1 copy-start.28
  533.7 75.9 %all-to-all-start.1 = ((bf16[16,48,2048]{2,1,0:T(8,128)(2,1)}), bf16[16,48,2048]{2,1,0:T(8,128)(2,1)S(1)}, u32[]{:S(2)}, u32[]{:S(2)}) async-start(bf16[16,48,2048]{2,1,0:T(8,128)(2,1)} %bitcast.310), calls=%async_computation.2 | async-start | bytes 6291456 | tf_op jit(solution)/shard_map/all_to_all | solution.py:246
  617.4 7.0 %copy-start.3 = (bf16[192,2048]{1,0:T(8,128)(2,1)S(1)}, bf16[192,2048]{1,0:T(8,128)(2,1)}, u32[]{:S(2)}) copy-start(bf16[192,2048]{1,0:T(8,128)(2,1)} %param.21) | copy-start | bytes 2359300
  617.4 7.0 %copy-start.4 = (bf16[192,2048]{1,0:T(8,128)(2,1)S(1)}, bf16[192,2048]{1,0:T(8,128)(2,1)}, u32[]{:S(2)}) copy-start(bf16[192,2048]{1,0:T(8,128)(2,1)} %reduce-scatter.2.cloned.1.call-done) | copy-start | bytes 2359300
  617.4 8.3 %copy-start.1 = (bf16[512,2048]{1,0:T(8,128)(2,1)S(1)}, bf16[512,2048]{1,0:T(8,128)(2,1)}, u32[]{:S(2)}) copy-start(bf16[512,2048]{1,0:T(8,128)(2,1)} %param.32) | copy-start | bytes 6291460
Sparse Core Ops, SparseCore 0:
  14.6 77.1 all-gather.14
  94.6 74.3 all-gather.16
  389.0 16.1 reduce-scatter.1
  406.6 21.0 all-gather.20
  429.1 21.0 all-gather.18
  451.5 21.0 all-gather.22
where the time goes:
time: 642 us; the launch traced here: 633 us
  blocking collectives  187 us (29%)
  other arithmetic  169 us (26%)
  waiting for transfers between devices  155 us (24%)
  matrix products  53.7 us (8%)
  local copies, waits for them, and re-layouts  38.6 us (6%)
  between operations  15.6 us (2%)
  starting transfers between devices  13.8 us (2%)
    all_gather x4, blocking collectives, carried_in(): everything = jax.tree.map(lambda part: lax.all_gather(part, axis), x)  155 us
    select_n x96, other arithmetic, lap(): return jax.tree.map(lambda a, b: jnp.where(reached, a, b), new, before)  118 us
    all_to_all x1, waiting for transfers between devices, body(): lax.all_to_all(answered, 'sp', split_axis=0, concat_axis=0, tiled=True)  69.6 us
    all_to_all x1, waiting for transfers between devices, body(): lax.all_to_all(outgoing, 'sp', split_axis=0, concat_axis=0, tiled=True)  68.9 us
    unnamed x1, blocking collectives  32.4 us
    exp x32, other arithmetic, combine(): earlier_weight = jnp.exp(earlier_peak + later_total - joined)  22 us
    reduce_scatter x1, waiting for transfers between devices, body(): lax.psum_scatter((jnp.dot(small_out, w_out_small, preferred_element_type=...  13 us
  transfers between devices with their start and end apart: 8, of which 4 were waited for; matrix products, arithmetic and copies ran while one was open for 9% of the time, Pallas kernels for 0%

commit v1 on v0

v1 whole, which is shorter than its diff:
```python
import functools

import jax
import jax.numpy as jnp
from jax import lax
from jax.experimental import pallas as pl
from jax.experimental.pallas import tpu as pltpu
from jax.sharding import PartitionSpec as P

floor_neg = -1e30
norm_eps = 1e-06
LANES = 128
MESH = pl.DeviceIdType.MESH
F32 = jnp.float32
BF16 = jnp.bfloat16


def iota(shape, axis):
    return lax.broadcasted_iota(jnp.int32, shape, axis)


def dot(a, b, ca=1, cb=0, **kw):
    return lax.dot_general(
        a, b, (((ca,), (cb,)), ((), ())), preferred_element_type=F32, **kw
    )


def exact_dot(a, b):
    return dot(a, b, precision=lax.Precision.HIGHEST)


def mixer_kernel(
    dims,
    qs, ks, vs, gs, ql, kl, vl, gl,
    lf, lft, li, lit,
    ws, wl, resid, gain, idt, wtt,
    after_ref, out_ref, comb_ref,
    tot_c, tot_a, pre_c, pre_a,
    send_c, send_a, recv_c, recv_a,
    inum, imax, iden, y, psend, precv, own,
    ssem_c, rsem_c, ssem_a, rsem_a, psem,
):
    steps, heads_s, heads_l, experts, capacity = dims
    length = qs.shape[0]
    per = heads_s * LANES // qs.shape[1]
    half = LANES // per
    pairs = heads_s // per
    units = pairs + heads_l
    rows = length // 2
    me = lax.axis_index("sp")
    core = lax.axis_index("tp")
    other = 1 - core

    def partner(step):
        bit = 1 << step
        upper = lax.rem(me // bit, 2)
        return me + bit * (1 - 2 * upper), upper

    barrier = pltpu.get_barrier_semaphore()
    for step in range(steps):
        pl.semaphore_signal(
            barrier, inc=1, device_id={"sp": partner(step)[0]}, device_id_type=MESH
        )
    pl.semaphore_signal(barrier, inc=1, device_id={"tp": other}, device_id_type=MESH)

    lane = iota((1, LANES), 1)

    def spread(columns):
        if len(columns) == 1:
            return jnp.broadcast_to(columns[0], (columns[0].shape[0], LANES))
        picked = columns[0]
        for i in range(1, len(columns)):
            picked = jnp.where(lane >= i * half, columns[i], picked)
        return picked

    def heads_of(unit):
        if unit < pairs:
            return list(range(unit * per, (unit + 1) * per))
        return [heads_s + unit - pairs]

    def view(small, large, unit):
        if unit < pairs:
            return small[:, unit * LANES : (unit + 1) * LANES]
        low = (unit - pairs) * LANES
        return large[:, low : low + LANES]

    def span(unit):
        if unit < pairs:
            return unit * half, half
        return pairs * half + (unit - pairs) * LANES, LANES

    tri = (iota((length, length), 0) >= iota((length, length), 1)).astype(F32)
    upper_tri = (iota((length, length), 0) <= iota((length, length), 1)).astype(F32)
    cum_col = exact_dot(tri, lf[...])
    u_row = lit[...] - exact_dot(lft[...], upper_tri)
    total = cum_col[length - 1 : length, :]
    grow = total - cum_col + li[...]
    peak = jnp.max(grow, axis=0, keepdims=True)
    factor = jnp.exp(grow - peak)

    for unit in range(units):
        hs = heads_of(unit)
        key = view(ks, kl, unit).astype(F32)
        scaled = spread([factor[:, h : h + 1] for h in hs]) * key
        full = dot(scaled.astype(BF16), view(vs, vl, unit), 0, 0)
        low, size = span(unit)
        if unit < pairs:
            packed = full[:half]
            for i in range(1, per):
                packed = jnp.where(lane >= i * half, full[i * half : (i + 1) * half], packed)
        else:
            packed = full
        tot_c[low : low + size, :] = packed
        tot_a[unit : unit + 1, :] = jnp.sum(scaled, axis=0, keepdims=True)
        tot_a[units + unit : units + unit + 1, :] = spread([peak[:, h : h + 1] for h in hs])
        tot_a[2 * units + unit : 2 * units + unit + 1, :] = spread(
            [total[:, h : h + 1] for h in hs]
        )
    pre_c[...] = jnp.zeros_like(pre_c)
    pre_a[...] = jnp.zeros_like(pre_a)
    pre_a[units : 2 * units, :] = jnp.full((units, LANES), floor_neg, F32)

    def copies(step):
        to = {"sp": partner(step)[0]}
        return (
            pltpu.make_async_remote_copy(
                send_c.at[step], recv_c.at[step], ssem_c.at[step], rsem_c.at[step],
                device_id=to, device_id_type=MESH,
            ),
            pltpu.make_async_remote_copy(
                send_a.at[step], recv_a.at[step], ssem_a.at[step], rsem_a.at[step],
                device_id=to, device_id_type=MESH,
            ),
        )

    def send(step):
        send_c[step] = tot_c[...].astype(BF16)
        send_a[step] = tot_a[...]
        for copy in copies(step):
            copy.start()

    def merge(early_c, early_a, late_c, late_a, out_c, out_a):
        em, eb = early_a[units : 2 * units, :], early_a[2 * units :, :]
        lm, lb = late_a[units : 2 * units, :], late_a[2 * units :, :]
        m = jnp.maximum(em + lb, lm)
        ew, lw = jnp.exp(em + lb - m), jnp.exp(lm - m)
        out_a[...] = jnp.concatenate(
            [ew * early_a[:units, :] + lw * late_a[:units, :], m, eb + lb], axis=0
        )
        for unit in range(units):
            low, size = span(unit)
            out_c[low : low + size, :] = (
                ew[unit : unit + 1] * early_c[low : low + size, :].astype(F32)
                + lw[unit : unit + 1] * late_c[low : low + size, :].astype(F32)
            )

    def receive(step):
        for copy in copies(step):
            copy.wait()
        upper = partner(step)[1]
        got_c, got_a = recv_c.at[step], recv_a.at[step]

        @pl.when(upper == 1)
        def _():
            merge(got_c, got_a[...], pre_c, pre_a[...], pre_c, pre_a)
            if step < steps - 1:
                merge(got_c, got_a[...], tot_c, tot_a[...], tot_c, tot_a)

        if step < steps - 1:

            @pl.when(upper == 0)
            def _():
                merge(tot_c, tot_a[...], got_c, got_a[...], tot_c, tot_a)

    block = LANES

    def inner(unit):
        hs = heads_of(unit)
        scale = (half if unit < pairs else LANES) ** (-0.5)
        q, k, v = view(qs, ql, unit), view(ks, kl, unit), view(vs, vl, unit)
        for start in range(0, length, block):
            width = start + block
            causal = iota((block, width), 1) <= iota((block, width), 0) + start
            nums, tops, dens = [], [], []
            for i, h in enumerate(hs):
                q_block = q[start : start + block]
                if len(hs) > 1:
                    mine = (lane >= i * half) & (lane < (i + 1) * half)
                    q_block = jnp.where(mine, q_block, jnp.zeros_like(q_block))
                raw = dot(q_block, k[:width], 1, 1) * scale
                masked = jnp.where(causal, u_row[h : h + 1, :width], floor_neg)
                top = jnp.max(masked, axis=1, keepdims=True)
                scored = raw * jnp.exp(masked - top)
                dens.append(jnp.sum(scored, axis=1, keepdims=True))
                tops.append(top)
                nums.append(dot(scored.astype(BF16), v[:width]))
            num = nums[0]
            for i in range(1, len(hs)):
                num = jnp.where(lane >= i * half, nums[i], num)
            inum[unit, start : start + block, :] = num
            imax[unit, start : start + block, :] = spread(tops)
            iden[unit, start : start + block, :] = spread(dens)

    pl.semaphore_wait(barrier, steps + 1)
    share = -(-units // steps)
    for step in range(steps):
        send(step)
        for unit in range(min(units, step * share), min(units, (step + 1) * share)):
            inner(unit)
        receive(step)

    for unit in range(units):
        hs = heads_of(unit)
        scale = (half if unit < pairs else LANES) ** (-0.5)
        low, size = span(unit)
        q = view(qs, ql, unit)
        state = pre_c[low : low + size, :]
        if unit < pairs:
            state = jnp.concatenate(
                [
                    jnp.where((lane >= i * half) & (lane < (i + 1) * half), state, 0.0)
                    for i in range(per)
                ],
                axis=0,
            )
        inter = dot(q, state.astype(BF16)) * scale
        qn = q.astype(F32) * pre_a[unit : unit + 1, :]
        if len(hs) > 1:
            parts = [
                jnp.sum(
                    jnp.where((lane >= i * half) & (lane < (i + 1) * half), qn, 0.0),
                    axis=1,
                    keepdims=True,
                )
                for i in range(per)
            ]
        else:
            parts = [jnp.sum(qn, axis=1, keepdims=True)]
        inter_den = spread(parts) * scale
        carry_m = pre_a[units + unit : units + unit + 1, :]
        top = jnp.maximum(carry_m, imax[unit])
        own_w, carry_w = jnp.exp(imax[unit] - top), jnp.exp(carry_m - top)
        numer = own_w * inum[unit] + carry_w * inter
        denom = own_w * iden[unit] + carry_w * inter_den
        memory = numer / jnp.maximum(jnp.abs(denom), 1.0)
        gate = jax.nn.sigmoid(view(gs, gl, unit).astype(F32))
        y[:, unit * LANES : (unit + 1) * LANES] = (gate * memory).astype(BF16)

    cut = qs.shape[1]
    features = ws.shape[1]
    step_n = 512

    def project(which, dst):
        low = pl.multiple_of(which * rows, 16)
        left = y[pl.ds(low, rows), :cut]
        right = y[pl.ds(low, rows), cut:]
        for n in range(0, features, step_n):
            dst[:, n : n + step_n] = (
                dot(left, ws[:, n : n + step_n]) + dot(right, wl[:, n : n + step_n])
            ).astype(BF16)

    project(other, psend)
    swap = pltpu.make_async_remote_copy(
        psend, precv, psem.at[0], psem.at[1], device_id={"tp": other}, device_id_type=MESH
    )
    swap.start()
    project(core, own)

    expert = iota((experts, rows), 0)
    first, second = idt[0:1, :] == expert, idt[1:2, :] == expert
    hit = (first | second).astype(BF16)
    weight = jnp.where(first, wtt[0:1, :], 0.0) + jnp.where(second, wtt[1:2, :], 0.0)
    before = (iota((rows, rows), 0) < iota((rows, rows), 1)).astype(BF16)
    count = dot(hit, before)
    slots = experts * capacity
    slot = iota((slots, 1), 0).astype(F32)
    group = jnp.floor((slot + 0.5) * (1.0 / capacity))
    place = slot - group * capacity
    member = (group == iota((slots, experts), 1).astype(F32)).astype(BF16)
    chosen = (dot(member, hit) > 0.5) & (dot(member, count.astype(BF16)) == place)
    select = chosen.astype(BF16)
    comb_ref[...] = jnp.where(chosen, dot(member, weight.astype(BF16)), 0.0).astype(BF16)

    swap.wait()
    after = resid[...].astype(F32) + (own[...].astype(F32) + precv[...].astype(F32))
    after_ref[...] = after
    normed = (
        after * lax.rsqrt(jnp.mean(after * after, axis=-1, keepdims=True) + norm_eps) * gain[...]
    ).astype(BF16)
    for n in range(0, features, step_n):
        out_ref[:, n : n + step_n] = dot(select, normed[:, n : n + step_n]).astype(BF16)


def mixer(args, experts, capacity):
    (resid, qs, ks, vs, ql, kl, vl, gs, gl, gates_s, gates_l, ws, wl, gain, ids, weights) = args
    length = qs.shape[0]
    heads_s, heads_l = gates_s.shape[2], gates_l.shape[2]
    steps = lax.axis_size("sp").bit_length() - 1
    gates = jnp.concatenate([gates_s, gates_l], axis=2)
    gates = jnp.pad(gates, ((0, 0), (0, 0), (0, -gates.shape[2] % 8)))
    li = gates[:, 0]
    lf = jax.nn.log_sigmoid(gates[:, 1]) + gates[:, 2]
    rows, features = resid.shape
    half = qs.shape[1] // heads_s
    pairs = qs.shape[1] // LANES
    units = pairs + heads_l
    state = pairs * half + heads_l * LANES
    vm = pl.BlockSpec(memory_space=pltpu.VMEM)
    slots = experts * capacity
    return pl.pallas_call(
        functools.partial(mixer_kernel, (steps, heads_s, heads_l, experts, capacity)),
        out_shape=(
            jax.ShapeDtypeStruct((rows, features), F32),
            jax.ShapeDtypeStruct((slots, features), BF16),
            jax.ShapeDtypeStruct((slots, rows), BF16),
        ),
        in_specs=[vm] * 18,
        out_specs=(vm, vm, vm),
        scratch_shapes=[
            pltpu.VMEM((state, LANES), F32),
            pltpu.VMEM((3 * units, LANES), F32),
            pltpu.VMEM((state, LANES), F32),
            pltpu.VMEM((3 * units, LANES), F32),
            pltpu.VMEM((steps, state, LANES), BF16),
            pltpu.VMEM((steps, 3 * units, LANES), F32),
            pltpu.VMEM((steps, state, LANES), BF16),
            pltpu.VMEM((steps, 3 * units, LANES), F32),
            pltpu.VMEM((units, length, LANES), F32),
            pltpu.VMEM((units, length, LANES), F32),
            pltpu.VMEM((units, length, LANES), F32),
            pltpu.VMEM((length, units * LANES), BF16),
            pltpu.VMEM((rows, features), BF16),
            pltpu.VMEM((rows, features), BF16),
            pltpu.VMEM((rows, features), BF16),
            pltpu.SemaphoreType.DMA((steps,)),
            pltpu.SemaphoreType.DMA((steps,)),
            pltpu.SemaphoreType.DMA((steps,)),
            pltpu.SemaphoreType.DMA((steps,)),
            pltpu.SemaphoreType.DMA((2,)),
        ],
        compiler_params=pltpu.CompilerParams(collective_id=0, has_side_effects=True),
        cost_estimate=pl.CostEstimate(
            flops=40_000_000_000, bytes_accessed=16_000_000, transcendentals=0
        ),
        name="mixer",
    )(
        qs, ks, vs, gs, ql, kl, vl, gl,
        lf, lf.T, li, li.T,
        ws, wl, resid, gain.reshape(1, -1), ids.T, weights.T,
    )


def expert_part(arrived, gate_w, up_w, down_w):
    gated = jnp.dot(arrived, gate_w, preferred_element_type=F32)
    lifted = jnp.dot(arrived, up_w, preferred_element_type=F32)
    hidden = (jax.nn.silu(gated) * lifted).astype(BF16)
    return jnp.dot(hidden, down_w, preferred_element_type=F32)


def body(*args):
    w_gate, w_up, w_down = args[16:]
    experts = w_gate.shape[0] * lax.axis_size("sp")
    tok_dev = args[1].shape[0]
    capacity = max(2, tok_dev * args[14].shape[1] // experts)
    own_w = (w_gate[0], w_up[0], w_down[0])
    swap = [(0, 1), (1, 0)]
    other_w = tuple(lax.ppermute(w, "tp", swap) for w in own_w)
    after, outgoing, comb = mixer(args[:16], experts, capacity)
    features = outgoing.shape[1]
    arrived = lax.all_to_all(
        outgoing.reshape(experts, capacity, features), "sp", 0, 0, tiled=True
    )
    flattened = arrived.reshape(-1, features)
    running = expert_part(flattened, *own_w) + expert_part(flattened, *other_w)
    answered = running.astype(BF16).reshape(arrived.shape)
    returned = lax.all_to_all(answered, "sp", 0, 0, tiled=True).reshape(-1, features)
    combined = lax.dot_general(
        comb, returned, (((0,), (0,)), ((), ())), preferred_element_type=F32
    )
    return (after + combined).astype(BF16)


def solution(mesh):
    return jax.shard_map(
        body,
        mesh=mesh,
        in_specs=(
            P(("sp", "tp"), None),
            P("sp", "tp"),
            P("sp", "tp"),
            P("sp", "tp"),
            P("sp", "tp"),
            P("sp", "tp"),
            P("sp", "tp"),
            P("sp", "tp"),
            P("sp", "tp"),
            P("sp", None, "tp"),
            P("sp", None, "tp"),
            P("tp", None),
            P("tp", None),
            P(),
            P(("sp", "tp"), None),
            P(("sp", "tp"), None),
            P("sp", None, "tp"),
            P("sp", None, "tp"),
            P("sp", "tp", None),
        ),
        out_specs=P(("sp", "tp"), None),
        check_vma=False,
    )
```

time: 642 us -> 244 us (0.38); the launches traced: 633 us -> 242 us
  other arithmetic: 169 us -> 1.44 us
  blocking collectives: 187 us -> 76.1 us
  waiting for transfers between devices: 155 us -> 71.6 us
  Pallas kernels: 0 us -> 37.3 us
  local copies, waits for them, and re-layouts: 38.6 us -> 2.23 us
  between operations: 15.6 us -> 0.03 us
  matrix products: 53.7 us -> 43.2 us
    all_gather x4 -> x0, blocking collectives: 155 us -> none  [carried_in(): everything = jax.tree.map(lambda part: lax.all_gather(part, axis), x)]
    select_n x98 -> x0, other arithmetic: 118 us -> none  [the longest x96 118 us: lap(): return jax.tree.map(lambda a, b: jnp.where(reached, a, b), new, before)]
    all_to_all x0 -> x1, blocking collectives: none -> 76.1 us  [body(): lax.all_to_all(answered, 'sp', 0, 0, tiled=True).reshape(-1, features)]
    all_to_all x2 -> x1, waiting for transfers between devices: 139 us -> 71.6 us  [body(): lax.all_to_all(outgoing.reshape(experts, capacity, features), 'sp', 0, 0,...]
    pallas_call x0 -> x1, Pallas kernels: none -> 37.3 us  [mixer(): pl.pallas_call(functools.partial(mixer_kernel, (steps, heads_s, heads_l,...]
    unnamed x1 -> x0, blocking collectives: 32.4 us -> none
    exp x34 -> x0, other arithmetic: 22.8 us -> none  [the longest x32 22 us: combine(): earlier_weight = jnp.exp(earlier_peak + later_total - joined)]
    reduce_scatter x1 -> x0, waiting for transfers between devices: 13 us -> none  [body(): lax.psum_scatter((jnp.dot(small_out, w_out_small, preferred_element_type=...]
  transfers between devices with their start and end apart: 8 -> 4, of which waited for: 4 -> 1; matrix products, arithmetic and copies ran while one was open for 9% -> 12% of each run, Pallas kernels for 0% -> 0%
where the time goes in v1:
time: 244 us; the launch traced here: 242 us
  blocking collectives  76.1 us (31%)
  waiting for transfers between devices  71.6 us (29%)
  matrix products  43.2 us (18%)
  Pallas kernels  37.3 us (15%)
  starting transfers between devices  9.72 us (4%)
    all_to_all x1, blocking collectives, body(): lax.all_to_all(answered, 'sp', 0, 0, tiled=True).reshape(-1, features)  76.1 us
    all_to_all x1, waiting for transfers between devices, body(): lax.all_to_all(outgoing.reshape(experts, capacity, features), 'sp', 0, 0,...  71.6 us
    pallas_call x1, Pallas kernels, mixer(): pl.pallas_call(functools.partial(mixer_kernel, (steps, heads_s, heads_l,...  37.3 us
    dot_general x2, matrix products, expert_part(): return jnp.dot(hidden, down_w, preferred_element_type=F32)  27.1 us
    dot_general x2, matrix products, expert_part(): gated = jnp.dot(arrived, gate_w, preferred_element_type=F32)  14.4 us
    all_to_all x1, starting transfers between devices, body(): lax.all_to_all(outgoing.reshape(experts, capacity, features), 'sp', 0, 0,...  9.12 us
  transfers between devices with their start and end apart: 4, of which 1 were waited for; matrix products, arithmetic and copies ran while one was open for 12% of the time, Pallas kernels for 0%

profile of v1, /device:TPU:12, one launch (start us, length us, event | category | flops | bytes accessed | tf_op | source)
XLA Modules:
  0.0 241.5 jit_solution(10041524341134123337)
XLA Ops:
  0.0 0.8 select_maximum_fusion
  0.8 0.6 fusion.25.lft
  1.4 0.6 slice_bitcast_fusion.1
  2.1 0.8 copy.20.lf
  2.9 0.8 copy.21.li
  3.7 37.3 %mixer.1 = (f32[192,2048]{1,0:T(8,128)}, bf16[768,2048]{1,0:T(8,128)(2,1)}, bf16[768,192]{1,0:T(8,128)(2,1)}) custom-call(bf16[384,512]{1,0:T(8,128)(2,1)} %qs.1, bf16[384,512]{1,0:T(8,128)(2,1)} %ks.1, bf16[384,512]{1,0:T(8,128)(2,1)} %vs.1, bf16[384,512]{1,0:T(8,128)(2,1)} %gs.1, bf16[384,512]{1,0:T(8,128)(2,1)} %ql.1, bf16[384,512]{1,0:T(8,128)(2,1)} %kl.1, ...), custom_call_target="tpu_custom_call" | custom-call | flops 40000000000 | bytes 16000000 | tf_op jit(solution)/shard_map/mixer/pallas_call | solution.py:310
  40.9 9.1 %all-to-all-start = ((bf16[16,48,2048]{2,1,0:T(8,128)(2,1)}), bf16[16,48,2048]{2,1,0:T(8,128)(2,1)S(1)}, u32[]{:S(2)}, u32[]{:S(2)}) async-start(bf16[16,48,2048]{2,1,0:T(8,128)(2,1)} %bitcast.50), calls=%async_computation | async-start | bytes 6291456 | tf_op jit(solution)/shard_map/all_to_all | solution.py:370
  50.1 0.1 collective-permute-start
  50.1 0.4 collective-permute-start.2
  50.6 0.1 collective-permute-start.1
  50.7 71.6 %all-to-all-done = bf16[16,48,2048]{2,1,0:T(8,128)(2,1)S(1)} async-done(((bf16[16,48,2048]{2,1,0:T(8,128)(2,1)}), bf16[16,48,2048]{2,1,0:T(8,128)(2,1)S(1)}, u32[]{:S(2)}, u32[]{:S(2)}) %all-to-all-start) | async-done | bytes 3145760 | tf_op jit(solution)/shard_map/all_to_all | solution.py:370
  122.2 7.2 %fusion.9 = f32[768,1024]{1,0:T(8,128)} fusion(bf16[768,2048]{1,0:T(8,128)(2,1)S(1)} %bitcast.46, bf16[1,2048,1024]{2,1,0:T(8,128)(2,1)} %param.35), kind=kOutput, calls=%fused_computation.19 | convolution fusion | flops 3221225472 | bytes 10485760 | tf_op jit(solution)/shard_map/dot_general | solution.py:354
  129.4 0.0 collective-permute-done
  129.4 7.2 %fusion.15 = f32[768,1024]{1,0:T(8,128)} fusion(bf16[768,2048]{1,0:T(8,128)(2,1)S(1)} %bitcast.47, bf16[2048,1024]{1,0:T(8,128)(2,1)} %collective-permute-done), kind=kOutput, calls=%fused_computation.24 | convolution fusion | flops 3221225472 | bytes 10485760 | tf_op jit(solution)/shard_map/dot_general | solution.py:354
  136.7 13.8 %fusion.2 = f32[768,2048]{1,0:T(8,128)} fusion(f32[768,1024]{1,0:T(8,128)} %fusion.9, bf16[768,2048]{1,0:T(8,128)(2,1)S(1)} %bitcast.48, bf16[1,1024,2048]{2,1,0:T(8,128)(2,1)} %param.37, bf16[1,2048,1024]{2,1,0:T(8,128)(2,1)} %param.36), kind=kOutput, calls=%fused_computation.6 | convolution fusion | flops 6447169536 | bytes 20971520 | tf_op jit(solution)/shard_map/dot_general | solution.py:357
  150.5 0.0 collective-permute-done.2
  150.5 0.0 collective-permute-done.1
  150.5 13.3 %add_convert_fusion = bf16[768,2048]{1,0:T(8,128)(2,1)} fusion(f32[768,2048]{1,0:T(8,128)} %fusion.2, bf16[1024,2048]{1,0:T(8,128)(2,1)} %collective-permute-done.2, f32[768,1024]{1,0:T(8,128)} %fusion.15, bf16[768,2048]{1,0:T(8,128)(2,1)S(1)} %bitcast.49, bf16[2048,1024]{1,0:T(8,128)(2,1)} %collective-permute-done.1), kind=kOutput, calls=%fused_computation | convolution fusion | flops 6450315264 | bytes 24117248 | tf_op jit(solution)/shard_map/dot_general | solution.py:357
  163.7 0.0 copy-start
  163.8 0.0 copy-start.1
  163.8 76.1 %all_to_all.10 = bf16[16,48,2048]{2,1,0:T(8,128)(2,1)S(1)} all-to-all(bf16[16,48,2048]{2,1,0:T(8,128)(2,1)} %bitcast.51), channel_id=1, replica_groups=mesh['sp'=16,'tp'=2] {'sp'}, dimensions={0} | all-to-all | bytes 6291456 | tf_op jit(solution)/shard_map/all_to_all | solution.py:376
  239.8 0.0 copy-done
  239.8 0.0 copy-done.1
  239.8 1.7 fusion
  (1 shorter events, 0.0 us)
Async XLA Ops:
  40.9 81.3 %all-to-all-start = ((bf16[16,48,2048]{2,1,0:T(8,128)(2,1)}), bf16[16,48,2048]{2,1,0:T(8,128)(2,1)S(1)}, u32[]{:S(2)}, u32[]{:S(2)}) async-start(bf16[16,48,2048]{2,1,0:T(8,128)(2,1)} %bitcast.50), calls=%async_computation | async-start | bytes 6291456 | tf_op jit(solution)/shard_map/all_to_all | solution.py:370
  50.1 79.4 %collective-permute-start = (bf16[2048,1024]{1,0:T(8,128)(2,1)}, bf16[2048,1024]{1,0:T(8,128)(2,1)}, u32[]{:S(2)}, u32[]{:S(2)}) collective-permute-start(bf16[2048,1024]{1,0:T(8,128)(2,1)} %bitcast.52), channel_id=1, source_target_pairs={{0,1},{1,0},{2,3},{3,2},{4,5},{5,4},{6,7},{7,6},{8,9},{9,8},{10,11... | collective-permute-start | bytes 12582920 | tf_op jit(solution)/shard_map/ppermute | solution.py:367
  50.1 100.3 %collective-permute-start.2 = (bf16[1024,2048]{1,0:T(8,128)(2,1)}, bf16[1024,2048]{1,0:T(8,128)(2,1)}, u32[]{:S(2)}, u32[]{:S(2)}) collective-permute-start(bf16[1024,2048]{1,0:T(8,128)(2,1)} %bitcast.53), channel_id=1, source_target_pairs={{0,1},{1,0},{2,3},{3,2},{4,5},{5,4},{6,7},{7,6},{8,9},{9,8},{10,11... | collective-permute-start | bytes 12582920 | tf_op jit(solution)/shard_map/ppermute | solution.py:367
  50.6 99.9 %collective-permute-start.1 = (bf16[2048,1024]{1,0:T(8,128)(2,1)}, bf16[2048,1024]{1,0:T(8,128)(2,1)}, u32[]{:S(2)}, u32[]{:S(2)}) collective-permute-start(bf16[2048,1024]{1,0:T(8,128)(2,1)} %bitcast.54), channel_id=1, source_target_pairs={{0,1},{1,0},{2,3},{3,2},{4,5},{5,4},{6,7},{7,6},{8,9},{9,8},{10,11... | collective-permute-start | bytes 12582920 | tf_op jit(solution)/shard_map/ppermute | solution.py:367
  163.7 76.1 %copy-start = (f32[192,2048]{1,0:T(8,128)S(1)}, f32[192,2048]{1,0:T(8,128)}, u32[]{:S(2)}) copy-start(f32[192,2048]{1,0:T(8,128)} %get-tuple-element.8) | copy-start | bytes 4718596
  163.8 76.1 %copy-start.1 = (bf16[768,192]{1,0:T(8,128)(2,1)S(1)}, bf16[768,192]{1,0:T(8,128)(2,1)}, u32[]{:S(2)}) copy-start(bf16[768,192]{1,0:T(8,128)(2,1)} %get-tuple-element.9) | copy-start | bytes 884740
